TPU v7x, 512 devices: a whole 4x4x16 slice. The times are simulated.
512 devices in a mesh: kv: 16 (over y, x), tp: 32 (over z, core).
Axes of the slice: x: 4, y: 4, z: 16, core: 2. Of those that a mesh axis runs over, the one named last changes fastest.
Arguments:
- tokens: bfloat16 [128, 4096], P(None, ('kv', 'tp')), may hold values from -60 to 60, as said below
- gain_mix: float32 [4096], replicated, may hold values from 0.1 to 1.9
- w_query: bfloat16 [4096, 4096], P('kv', 'tp'), may hold values from -0.09375 to 0.09375
- w_key: bfloat16 [4096, 4096], P('kv', 'tp'), may hold values from -0.75 to 0.75
- w_value: bfloat16 [4096, 4096], P('kv', 'tp'), may hold values from -0.09375 to 0.09375
- w_outgate: bfloat16 [4096, 4096], P('kv', 'tp'), may hold values from -0.09375 to 0.09375
- w_gates: bfloat16 [4096, 32], P('kv'), may hold values from -0.09375 to 0.09375
- forget_bias: float32 [16], replicated, may hold values from 0 to 4
- cell_state: float32 [128, 4096, 256], P('kv', 'tp'), may hold values from -1.5 to 1.5
- norm_state: float32 [128, 16, 256], P('kv'), may hold values from -1.5 to 1.5
- max_state: float32 [128, 16], P('kv'), may hold values from -1 to 2
- gain_group: float32 [4096], replicated, may hold values from 0.1 to 1.9
- w_mix: bfloat16 [4096, 4096], P('tp', 'kv'), may hold values from -0.1875 to 0.1875
- gain_ffn: float32 [4096], replicated, may hold values from 0.1 to 1.9
- w_up: bfloat16 [4096, 16384], P('kv', 'tp'), may hold values from -0.09375 to 0.09375
- w_down: bfloat16 [16384, 4096], P('tp', 'kv'), may hold values from -0.09375 to 0.09375
Outputs:
- layer_out: bfloat16 [128, 4096], P(None, ('kv', 'tp'))
- cell_next: float32 [128, 4096, 256], P('kv', 'tp')
- norm_next: float32 [128, 16, 256], P('kv')
- max_next: float32 [128, 16], P('kv')
Inputs may be any that keep to these rules, and one draw needn't show every extreme that they name: `tokens`: finite activations.
All inputs are finite; a program needn't handle non-finite values.
Results may differ from a plain program's by a relative error of at most 0.019.
Values may be sent and summed in bfloat16 or wider, within the bound.
A program may use at most 64 MiB of HBM per device.

v0:
```python
import functools
import math

import jax
import jax.numpy as jnp
from jax import lax
from jax.sharding import Mesh
from jax.sharding import PartitionSpec as P

KV = ("kv_0", "kv_1")
KV_TP = ("kv_0", "kv_1", "tp")


EPSILON = 1e-06


def from_everyone(array, axis):
    copies = jnp.broadcast_to(array, (lax.axis_size(axis), *array.shape))
    return lax.all_to_all(copies, axis, split_axis=0, concat_axis=0, tiled=True)


def in_order(blocks, dim):
    lengths = list(blocks.shape[1:])
    lengths[dim] *= blocks.shape[0]
    return jnp.moveaxis(blocks, 0, dim).reshape(lengths)


def gathered_copies(array, axis, dim):
    blocks = from_everyone(array, axis)
    return in_order(blocks, dim)


def split_up(array, dim, length):
    lengths = array.shape
    blocks = array.reshape(*lengths[:dim], length, lengths[dim] // length, *lengths[dim + 1 :])
    return jnp.moveaxis(blocks, dim, 0)


def sum_at_owner(array, axis, dim):
    length = lax.axis_size(axis)
    blocks = lax.all_to_all(split_up(array, dim, length), axis, 0, 0, tiled=True)
    return jnp.sum(blocks.astype(jnp.float32), axis=0)


def as_sent(array):

    def short(part):
        return part.astype(jnp.bfloat16) if part.dtype == jnp.float32 else part

    return jax.tree.map(short, array)


def in_one_piece(arrays, axis, dim, along):
    both = jnp.concatenate(arrays, axis=along)
    whole, at, outs = (lax.all_gather(both, axis, axis=dim, tiled=True), 0, [])
    for a in arrays:
        outs.append(lax.slice_in_dim(whole, at, at + a.shape[along], axis=along))
        at += a.shape[along]
    return tuple(outs)


def over_copies(array, axis):
    everything = from_everyone(array, axis)
    return jnp.sum(everything, axis=0)


def summed_on_arrival(array, axis, dim):
    length = lax.axis_size(axis)
    blocks = lax.all_to_all(split_up(array, dim, length), axis, 0, 0, tiled=True)
    return jnp.sum(blocks, axis=0)


def one_axis_at_a_time(array, axes):
    return functools.reduce(lax.psum, axes, array)


def per_device(
    tokens,
    gain_mix,
    w_query,
    w_key,
    w_value,
    w_outgate,
    w_gates,
    forget_bias,
    cell_state,
    norm_state,
    max_state,
    gain_group,
    w_mix,
    gain_ffn,
    w_up,
    w_down,
):
    f32 = jnp.float32
    bf16 = jnp.bfloat16
    exact = lax.Precision.HIGHEST
    width = gain_mix.shape[0]
    kv_index = lax.axis_index(KV)
    tp_index = lax.axis_index("tp")
    tokf = tokens.astype(f32)
    block_rows = gathered_copies(tokens, "tp", 1)
    block = block_rows.shape[1]
    blockf = block_rows.astype(f32)
    gain_block = lax.dynamic_slice_in_dim(gain_mix, kv_index * block, block)
    normed = (blockf * gain_block).astype(bf16)
    partials = tuple(
        (
            jnp.dot(normed, weight, preferred_element_type=f32)
            for weight in (w_query, w_key, w_value, w_outgate, w_gates)
        )
    )
    partials = partials + (jnp.sum(blockf * blockf, axis=1),)
    summed = jax.tree.map(lambda part: sum_at_owner(part, KV, 0), as_sent(partials))
    seqs = summed[0].shape[0]
    seq_squares = summed[5]
    scale_in = lax.rsqrt(seq_squares / width + EPSILON)[:, None]
    query_part = (summed[0] * scale_in).astype(bf16)
    key_part = (summed[1] * scale_in).astype(bf16)
    values = summed[2] * scale_in
    gate_out = summed[3] * scale_in
    gates = summed[4] * scale_in
    query_all, key_all = in_one_piece((query_part, key_part), "tp", 1, 0)
    heads = forget_bias.shape[0]
    head_dim = cell_state.shape[2]
    value_rows = cell_state.shape[1]
    queryf = query_all.astype(f32).reshape(seqs, heads, head_dim)
    keyf = key_all.astype(f32).reshape(seqs, heads, head_dim) / math.sqrt(head_dim)
    gate_in = gates[:, :heads]
    log_forget = jax.nn.log_sigmoid(gates[:, heads:] + forget_bias)
    max_next = jnp.maximum(log_forget + max_state, gate_in)
    decay = jnp.exp(log_forget + max_state - max_next)
    inflow = jnp.exp(gate_in - max_next)
    norm_next = decay[..., None] * norm_state + inflow[..., None] * keyf
    denom_heads = jnp.maximum(jnp.abs(jnp.sum(norm_next * queryf, axis=2)), 1.0)
    row_ids = tp_index * value_rows + jnp.arange(value_rows)
    select = (row_ids[:, None] // head_dim == jnp.arange(heads)[None, :]).astype(f32)
    query_rows = jnp.einsum("shd,rh->srd", queryf, select, precision=exact)
    key_rows = jnp.einsum("shd,rh->srd", keyf, select, precision=exact)
    decay_rows = jnp.einsum("sh,rh->sr", decay, select, precision=exact)
    inflow_rows = jnp.einsum("sh,rh->sr", inflow, select, precision=exact)
    denom_rows = jnp.einsum("sh,rh->sr", denom_heads, select, precision=exact)
    cell_next = (
        decay_rows[:, :, None] * cell_state
        + inflow_rows[:, :, None] * values[:, :, None] * key_rows
    )
    numer = jnp.sum(cell_next * query_rows, axis=2)
    cell_read = (jax.nn.sigmoid(gate_out) * (numer / denom_rows)).astype(bf16)
    read_rows = gathered_copies(cell_read, KV, 0)
    readf = read_rows.astype(f32)
    group_total = over_copies(jnp.sum(readf * readf, axis=1), "tp")
    scale_group = lax.rsqrt(group_total / (heads * head_dim) + EPSILON)[:, None]
    gain_rows = lax.dynamic_slice_in_dim(gain_group, tp_index * value_rows, value_rows)
    grouped = (readf * gain_rows).astype(bf16)
    mix_terms = jnp.dot(grouped, w_mix, preferred_element_type=f32)
    mix_summed = summed_on_arrival(mix_terms, "tp", 1)
    mixed = (tokf + mix_summed * scale_group).astype(bf16)
    ffn_block = w_up.shape[0]
    piece = gathered_copies(mixed, "tp", 1)
    count = piece.shape[1]
    piecef = piece.astype(f32)
    gain_piece = lax.dynamic_slice_in_dim(gain_ffn, kv_index * ffn_block, count)
    normed_piece = (piecef * gain_piece).astype(bf16)
    up_part = jnp.dot(normed_piece, w_up, preferred_element_type=f32)
    square_part = jnp.sum(piecef * piecef, axis=1)
    up_share = sum_at_owner(up_part.astype(jnp.bfloat16), KV, 1)
    square_total = one_axis_at_a_time(square_part, KV)
    scale_ffn = lax.rsqrt(square_total / width + EPSILON)[:, None]
    hidden_share = jnp.square(jax.nn.relu(up_share * scale_ffn)).astype(bf16)
    hidden = gathered_copies(hidden_share, KV, 1)
    down_terms = jnp.dot(hidden, w_down, preferred_element_type=f32)
    ffn_summed = summed_on_arrival(down_terms, "tp", 1)
    layer_out = (mixed.astype(f32) + ffn_summed).astype(bf16)
    return (layer_out, cell_next, norm_next, max_next)


def solution(mesh):
    split = Mesh(mesh.devices.reshape(4, 4, mesh.shape["tp"]), ("kv_0", "kv_1", "tp"))
    in_specs = (
        P(None, KV_TP),
        P(),
        P(KV, "tp"),
        P(KV, "tp"),
        P(KV, "tp"),
        P(KV, "tp"),
        P(KV, None),
        P(),
        P(KV, "tp", None),
        P(KV, None, None),
        P(KV, None),
        P(),
        P("tp", KV),
        P(),
        P(KV, "tp"),
        P("tp", KV),
    )
    out_specs = (P(None, KV_TP), P(KV, "tp", None), P(KV, None, None), P(KV, None))
    return jax.shard_map(
        per_device, mesh=split, in_specs=in_specs, out_specs=out_specs, check_vma=False
    )
```

profile of v0, /device:TPU:1, one launch (start us, length us, event | category | flops | bytes accessed | tf_op | source)
XLA Modules:
  0.0 257.2 jit_solution(8622874492189523639)
XLA Ops:
  0.6 1.4 broadcast_in_dim.12
  2.0 16.7 %all-to-all-start = ((bf16[32,128,8]{1,2,0:T(8,128)(2,1)}), bf16[32,128,8]{1,2,0:T(8,128)(2,1)S(1)}, u32[]{:S(2)}, u32[]{:S(2)}) async-start(bf16[32,128,8]{1,2,0:T(8,128)(2,1)} %broadcast_in_dim.12), calls=%async_computation | async-start | bytes 131072 | tf_op jit(solution)/shard_map/all_to_all | solution.py:19
  18.8 0.8 dynamic_slice.9
  19.6 12.2 %all-to-all-done = bf16[32,128,8]{1,2,0:T(8,128)(2,1)S(1)} async-done(((bf16[32,128,8]{1,2,0:T(8,128)(2,1)}), bf16[32,128,8]{1,2,0:T(8,128)(2,1)S(1)}, u32[]{:S(2)}, u32[]{:S(2)}) %all-to-all-start) | async-done | bytes 65568 | tf_op jit(solution)/shard_map/all_to_all | solution.py:19
  31.8 0.7 convert_element_type.164
  32.5 6.8 %all-to-all-start.2 = ((bf16[16,1,8]{2,1,0:T(2,128)(2,1)}), bf16[16,1,8]{2,1,0:T(2,128)(2,1)S(1)}, u32[]{:S(2)}, u32[]{:S(2)}) async-start(bf16[16,1,8]{2,1,0:T(2,128)(2,1)} %convert_element_type.164), calls=%async_computation.2 | async-start | bytes 16384 | tf_op jit(solution)/shard_map/all_to_all | solution.py:41
  39.3 0.9 fusion.7
  40.2 0.9 fusion.6
  41.3 0.6 copy-done.7
  41.9 0.9 fusion.5
  42.8 0.9 fusion.4
  43.9 0.7 reshape.158
  44.6 1.2 all-to-all-done.2
  45.7 5.5 %all-to-all-start.3 = ((bf16[16,2,128]{2,1,0:T(2,128)(2,1)}), bf16[16,2,128]{2,1,0:T(2,128)(2,1)S(1)}, u32[]{:S(2)}, u32[]{:S(2)}) async-start(bf16[16,2,128]{2,1,0:T(2,128)(2,1)} %reshape.158), calls=%async_computation.3 | async-start | bytes 16384 | tf_op jit(solution)/shard_map/all_to_all | solution.py:41
  51.3 6.2 %all-to-all-done.3 = bf16[16,2,128]{2,1,0:T(2,128)(2,1)S(1)} async-done(((bf16[16,2,128]{2,1,0:T(2,128)(2,1)}), bf16[16,2,128]{2,1,0:T(2,128)(2,1)S(1)}, u32[]{:S(2)}, u32[]{:S(2)}) %all-to-all-start.3) | async-done | bytes 8224 | tf_op jit(solution)/shard_map/all_to_all | solution.py:41
  57.5 3.5 %all-to-all-start.6 = ((bf16[16,8,128]{2,1,0:T(8,128)(2,1)}), bf16[16,8,128]{2,1,0:T(8,128)(2,1)S(1)}, u32[]{:S(2)}, u32[]{:S(2)}) async-start(bf16[16,8,128]{2,1,0:T(8,128)(2,1)} %fusion.7), calls=%async_computation.6 | async-start | bytes 65536 | tf_op jit(solution)/shard_map/all_to_all | solution.py:41
  61.5 5.9 %all-to-all-done.6 = bf16[16,8,128]{2,1,0:T(8,128)(2,1)S(1)} async-done(((bf16[16,8,128]{2,1,0:T(8,128)(2,1)}), bf16[16,8,128]{2,1,0:T(8,128)(2,1)S(1)}, u32[]{:S(2)}, u32[]{:S(2)}) %all-to-all-start.6) | async-done | bytes 32800 | tf_op jit(solution)/shard_map/all_to_all | solution.py:41
  67.4 3.5 %all-to-all-start.5 = ((bf16[16,8,128]{2,1,0:T(8,128)(2,1)}), bf16[16,8,128]{2,1,0:T(8,128)(2,1)S(1)}, u32[]{:S(2)}, u32[]{:S(2)}) async-start(bf16[16,8,128]{2,1,0:T(8,128)(2,1)} %fusion.6), calls=%async_computation.5 | async-start | bytes 65536 | tf_op jit(solution)/shard_map/all_to_all | solution.py:41
  70.9 6.4 %all-to-all-done.5 = bf16[16,8,128]{2,1,0:T(8,128)(2,1)S(1)} async-done(((bf16[16,8,128]{2,1,0:T(8,128)(2,1)}), bf16[16,8,128]{2,1,0:T(8,128)(2,1)S(1)}, u32[]{:S(2)}, u32[]{:S(2)}) %all-to-all-start.5) | async-done | bytes 32800 | tf_op jit(solution)/shard_map/all_to_all | solution.py:41
  77.3 3.5 %all-to-all-start.4 = ((bf16[16,8,128]{2,1,0:T(8,128)(2,1)}), bf16[16,8,128]{2,1,0:T(8,128)(2,1)S(1)}, u32[]{:S(2)}, u32[]{:S(2)}) async-start(bf16[16,8,128]{2,1,0:T(8,128)(2,1)} %fusion.5), calls=%async_computation.4 | async-start | bytes 65536 | tf_op jit(solution)/shard_map/all_to_all | solution.py:41
  80.9 33.5 %all_gather.3 = bf16[16,4096]{1,0:T(8,128)(2,1)S(1)} all-gather(bf16[16,128]{1,0:T(8,128)(2,1)S(1)} %pad_maximum_fusion), channel_id=1, replica_groups=mesh['kv_0'=4,'kv_1'=4,'tp'=32] {'tp'}, dimensions={1}, use_global_device_ids=true | all-gather | bytes 135168 | tf_op jit(solution)/shard_map/all_gather | solution.py:55
  114.5 7.0 %all-to-all-start.1 = ((bf16[16,8,128]{2,1,0:T(8,128)(2,1)}), bf16[16,8,128]{2,1,0:T(8,128)(2,1)S(1)}, u32[]{:S(2)}, u32[]{:S(2)}) async-start(bf16[16,8,128]{2,1,0:T(8,128)(2,1)} %fusion.4), calls=%async_computation.1 | async-start | bytes 65536 | tf_op jit(solution)/shard_map/all_to_all | solution.py:41
  121.7 0.8 multiply_reduce_fusion
  122.4 0.7 fusion.2
  123.6 4.4 %all-to-all-done.1 = bf16[16,8,128]{2,1,0:T(8,128)(2,1)S(1)} async-done(((bf16[16,8,128]{2,1,0:T(8,128)(2,1)}), bf16[16,8,128]{2,1,0:T(8,128)(2,1)S(1)}, u32[]{:S(2)}, u32[]{:S(2)}) %all-to-all-start.1) | async-done | bytes 32800 | tf_op jit(solution)/shard_map/all_to_all | solution.py:41
  128.1 0.6 broadcast_in_dim.13
  128.7 3.5 %all-to-all-start.7 = ((bf16[16,8,128]{2,1,0:T(8,128)(2,1)}), bf16[16,8,128]{2,1,0:T(8,128)(2,1)S(1)}, u32[]{:S(2)}, u32[]{:S(2)}) async-start(bf16[16,8,128]{2,1,0:T(8,128)(2,1)} %broadcast_in_dim.13), calls=%async_computation.7 | async-start | bytes 65536 | tf_op jit(solution)/shard_map/all_to_all | solution.py:19
  132.3 0.8 dynamic_slice.10
  133.1 5.5 %all-to-all-done.7 = bf16[16,8,128]{2,1,0:T(8,128)(2,1)S(1)} async-done(((bf16[16,8,128]{2,1,0:T(8,128)(2,1)}), bf16[16,8,128]{2,1,0:T(8,128)(2,1)S(1)}, u32[]{:S(2)}, u32[]{:S(2)}) %all-to-all-start.7) | async-done | bytes 32800 | tf_op jit(solution)/shard_map/all_to_all | solution.py:19
  138.8 0.6 broadcast_in_dim.15
  139.4 7.4 %all-to-all-start.9 = ((f32[32,1,128]{2,1,0:T(1,128)}), f32[32,1,128]{2,1,0:T(1,128)S(1)}, u32[]{:S(2)}, u32[]{:S(2)}) async-start(f32[32,1,128]{2,1,0:T(1,128)} %broadcast_in_dim.15), calls=%async_computation.9 | async-start | bytes 32768 | tf_op jit(solution)/shard_map/all_to_all | solution.py:19
  147.0 0.7 copy.75
  147.7 10.9 %all-to-all-done.9 = f32[32,1,128]{2,1,0:T(1,128)S(1)} async-done(((f32[32,1,128]{2,1,0:T(1,128)}), f32[32,1,128]{2,1,0:T(1,128)S(1)}, u32[]{:S(2)}, u32[]{:S(2)}) %all-to-all-start.9) | async-done | bytes 16416 | tf_op jit(solution)/shard_map/all_to_all | solution.py:19
  158.6 4.4 %all-to-all-start.8 = ((f32[32,128,8]{1,2,0:T(8,128)}), f32[32,128,8]{1,2,0:T(8,128)S(1)}, u32[]{:S(2)}, u32[]{:S(2)}) async-start(f32[32,128,8]{1,2,0:T(8,128)} %copy.75), calls=%async_computation.8 | async-start | bytes 262144 | tf_op jit(solution)/shard_map/all_to_all | solution.py:69
  163.1 16.2 %all-to-all-done.8 = f32[32,128,8]{1,2,0:T(8,128)S(1)} async-done(((f32[32,128,8]{1,2,0:T(8,128)}), f32[32,128,8]{1,2,0:T(8,128)S(1)}, u32[]{:S(2)}, u32[]{:S(2)}) %all-to-all-start.8) | async-done | bytes 131104 | tf_op jit(solution)/shard_map/all_to_all | solution.py:69
  179.3 0.6 broadcast_in_dim.16
  179.9 4.8 %all-to-all-start.10 = ((bf16[32,128,8]{1,2,0:T(8,128)(2,1)}), bf16[32,128,8]{1,2,0:T(8,128)(2,1)S(1)}, u32[]{:S(2)}, u32[]{:S(2)}) async-start(bf16[32,128,8]{1,2,0:T(8,128)(2,1)} %broadcast_in_dim.16), calls=%async_computation.10 | async-start | bytes 131072 | tf_op jit(solution)/shard_map/all_to_all | solution.py:19
  184.8 0.8 dynamic_slice.11
  185.5 12.3 %all-to-all-done.10 = bf16[32,128,8]{1,2,0:T(8,128)(2,1)S(1)} async-done(((bf16[32,128,8]{1,2,0:T(8,128)(2,1)}), bf16[32,128,8]{1,2,0:T(8,128)(2,1)S(1)}, u32[]{:S(2)}, u32[]{:S(2)}) %all-to-all-start.10) | async-done | bytes 65568 | tf_op jit(solution)/shard_map/all_to_all | solution.py:19
  198.1 0.7 copy.77
  198.8 3.5 %all-to-all-start.11 = ((bf16[16,128,32]{1,2,0:T(8,128)(2,1)}), bf16[16,128,32]{1,2,0:T(8,128)(2,1)S(1)}, u32[]{:S(2)}, u32[]{:S(2)}) async-start(bf16[16,128,32]{1,2,0:T(8,128)(2,1)} %bitcast.22), calls=%async_computation.11 | async-start | bytes 262144 | tf_op jit(solution)/shard_map/all_to_all | solution.py:41
  202.4 9.2 %psum.14 = f32[128]{0:T(128)S(1)} all-reduce(f32[128]{0:T(128)S(1)} %fusion.16), channel_id=1, replica_groups=mesh['kv_0'=4,'kv_1'=4,'tp'=32] {'kv_0'}, use_global_device_ids=true, to_apply=%region_14.15 | all-reduce | flops 128 | bytes 1024 | tf_op jit(solution)/shard_map/psum | solution.py:74
  211.6 8.0 %psum.15 = f32[128]{0:T(128)S(1)} all-reduce(f32[128]{0:T(128)S(1)} %psum.14), channel_id=1, replica_groups=mesh['kv_0'=4,'kv_1'=4,'tp'=32] {'kv_1'}, use_global_device_ids=true, to_apply=%region_15.16 | all-reduce | flops 128 | bytes 1024 | tf_op jit(solution)/shard_map/psum | solution.py:74
  219.7 0.7 broadcast_in_dim.17
  220.3 3.5 %all-to-all-start.12 = ((bf16[16,128,32]{1,2,0:T(8,128)(2,1)}), bf16[16,128,32]{1,2,0:T(8,128)(2,1)S(1)}, u32[]{:S(2)}, u32[]{:S(2)}) async-start(bf16[16,128,32]{1,2,0:T(8,128)(2,1)} %broadcast_in_dim.17), calls=%async_computation.12 | async-start | bytes 262144 | tf_op jit(solution)/shard_map/all_to_all | solution.py:19
  224.0 6.6 %all-to-all-done.12 = bf16[16,128,32]{1,2,0:T(8,128)(2,1)S(1)} async-done(((bf16[16,128,32]{1,2,0:T(8,128)(2,1)}), bf16[16,128,32]{1,2,0:T(8,128)(2,1)S(1)}, u32[]{:S(2)}, u32[]{:S(2)}) %all-to-all-start.12) | async-done | bytes 131104 | tf_op jit(solution)/shard_map/all_to_all | solution.py:19
  231.0 25.7 %all_to_all.72 = f32[32,128,8]{1,2,0:T(8,128)S(1)} all-to-all(f32[32,128,8]{1,2,0:T(8,128)S(1)} %copy.81), channel_id=1, replica_groups=mesh['kv_0'=4,'kv_1'=4,'tp'=32] {'tp'}, dimensions={0} | all-to-all | bytes 262144 | tf_op jit(solution)/shard_map/all_to_all | solution.py:69
  256.7 0.6 add_convert_fusion
  (71 shorter events, 3.2 us)
Async XLA Ops:
  0.6 197.2 %copy-start = (bf16[256,512]{1,0:T(8,128)(2,1)S(1)}, bf16[256,512]{1,0:T(8,128)(2,1)}, u32[]{:S(2)}) copy-start(bf16[256,512]{1,0:T(8,128)(2,1)} %param.30) | copy-start | bytes 786436
  2.0 29.8 %all-to-all-start = ((bf16[32,128,8]{1,2,0:T(8,128)(2,1)}), bf16[32,128,8]{1,2,0:T(8,128)(2,1)S(1)}, u32[]{:S(2)}, u32[]{:S(2)}) async-start(bf16[32,128,8]{1,2,0:T(8,128)(2,1)} %broadcast_in_dim.12), calls=%async_computation | async-start | bytes 131072 | tf_op jit(solution)/shard_map/all_to_all | solution.py:19
  18.8 20.5 %copy-start.5 = (bf16[256,128]{1,0:T(8,128)(2,1)S(1)}, bf16[256,128]{1,0:T(8,128)(2,1)}, u32[]{:S(2)}) copy-start(bf16[256,128]{1,0:T(8,128)(2,1)} %param.19) | copy-start | bytes 196612
  32.5 13.2 %all-to-all-start.2 = ((bf16[16,1,8]{2,1,0:T(2,128)(2,1)}), bf16[16,1,8]{2,1,0:T(2,128)(2,1)S(1)}, u32[]{:S(2)}, u32[]{:S(2)}) async-start(bf16[16,1,8]{2,1,0:T(2,128)(2,1)} %convert_element_type.164), calls=%async_computation.2 | async-start | bytes 16384 | tf_op jit(solution)/shard_map/all_to_all | solution.py:41
  39.3 0.9 copy-start.6
  40.2 0.9 copy-start.14
  41.1 0.8 copy-start.7
  41.1 1.7 copy-start.8
  41.1 20.1 %copy-start.10 = (f32[8,16]{1,0:T(8,128)S(1)}, f32[8,16]{1,0:T(8,128)}, u32[]{:S(2)}) copy-start(f32[8,16]{1,0:T(8,128)} %param.26) | copy-start | bytes 1540
  41.1 20.1 %copy-start.13 = (f32[16]{0:T(128)S(1)}, f32[16]{0:T(128)}, u32[]{:S(2)}) copy-start(f32[16]{0:T(128)} %param.23) | copy-start | bytes 196
  41.9 80.5 %copy-start.2 = (f32[8,128,256]{2,1,0:T(8,128)S(1)}, f32[8,128,256]{2,1,0:T(8,128)}, u32[]{:S(2)}) copy-start(f32[8,128,256]{2,1,0:T(8,128)} %param.24) | copy-start | bytes 3145732
  45.7 11.8 %all-to-all-start.3 = ((bf16[16,2,128]{2,1,0:T(2,128)(2,1)}), bf16[16,2,128]{2,1,0:T(2,128)(2,1)S(1)}, u32[]{:S(2)}, u32[]{:S(2)}) async-start(bf16[16,2,128]{2,1,0:T(2,128)(2,1)} %reshape.158), calls=%async_computation.3 | async-start | bytes 16384 | tf_op jit(solution)/shard_map/all_to_all | solution.py:41
  57.5 9.9 %all-to-all-start.6 = ((bf16[16,8,128]{2,1,0:T(8,128)(2,1)}), bf16[16,8,128]{2,1,0:T(8,128)(2,1)S(1)}, u32[]{:S(2)}, u32[]{:S(2)}) async-start(bf16[16,8,128]{2,1,0:T(8,128)(2,1)} %fusion.7), calls=%async_computation.6 | async-start | bytes 65536 | tf_op jit(solution)/shard_map/all_to_all | solution.py:41
  61.3 60.2 %copy-start.11 = (f32[8,16]{1,0:T(8,128)}, f32[8,16]{1,0:T(8,128)S(1)}, u32[]{:S(2)}) copy-start(f32[8,16]{1,0:T(8,128)S(1)} %get-tuple-element.7) | copy-start | bytes 1540
  67.4 9.9 %all-to-all-start.5 = ((bf16[16,8,128]{2,1,0:T(8,128)(2,1)}), bf16[16,8,128]{2,1,0:T(8,128)(2,1)S(1)}, u32[]{:S(2)}, u32[]{:S(2)}) async-start(bf16[16,8,128]{2,1,0:T(8,128)(2,1)} %fusion.6), calls=%async_computation.5 | async-start | bytes 65536 | tf_op jit(solution)/shard_map/all_to_all | solution.py:41
  77.3 37.2 %all-to-all-start.4 = ((bf16[16,8,128]{2,1,0:T(8,128)(2,1)}), bf16[16,8,128]{2,1,0:T(8,128)(2,1)S(1)}, u32[]{:S(2)}, u32[]{:S(2)}) async-start(bf16[16,8,128]{2,1,0:T(8,128)(2,1)} %fusion.5), calls=%async_computation.4 | async-start | bytes 65536 | tf_op jit(solution)/shard_map/all_to_all | solution.py:41
  114.5 7.2 %copy-start.4 = (f32[8,16,256]{2,1,0:T(8,128)S(1)}, f32[8,16,256]{2,1,0:T(8,128)}, u32[]{:S(2)}) copy-start(f32[8,16,256]{2,1,0:T(8,128)} %param.25) | copy-start | bytes 393220
  114.5 13.5 %all-to-all-start.1 = ((bf16[16,8,128]{2,1,0:T(8,128)(2,1)}), bf16[16,8,128]{2,1,0:T(8,128)(2,1)S(1)}, u32[]{:S(2)}, u32[]{:S(2)}) async-start(bf16[16,8,128]{2,1,0:T(8,128)(2,1)} %fusion.4), calls=%async_computation.1 | async-start | bytes 65536 | tf_op jit(solution)/shard_map/all_to_all | solution.py:41
  123.2 35.4 %copy-start.1 = (f32[8,128,256]{2,1,0:T(8,128)}, f32[8,128,256]{2,1,0:T(8,128)S(1)}, u32[]{:S(2)}) copy-start(f32[8,128,256]{2,1,0:T(8,128)S(1)} %fusion.2) | copy-start | bytes 3145732
  128.1 4.1 %copy-start.9 = (bf16[128,256]{1,0:T(8,128)(2,1)S(1)}, bf16[128,256]{1,0:T(8,128)(2,1)}, u32[]{:S(2)}) copy-start(bf16[128,256]{1,0:T(8,128)(2,1)} %param.28) | copy-start | bytes 196612
  128.7 9.9 %all-to-all-start.7 = ((bf16[16,8,128]{2,1,0:T(8,128)(2,1)}), bf16[16,8,128]{2,1,0:T(8,128)(2,1)S(1)}, u32[]{:S(2)}, u32[]{:S(2)}) async-start(bf16[16,8,128]{2,1,0:T(8,128)(2,1)} %broadcast_in_dim.13), calls=%async_computation.7 | async-start | bytes 65536 | tf_op jit(solution)/shard_map/all_to_all | solution.py:19
  139.4 19.2 %all-to-all-start.9 = ((f32[32,1,128]{2,1,0:T(1,128)}), f32[32,1,128]{2,1,0:T(1,128)S(1)}, u32[]{:S(2)}, u32[]{:S(2)}) async-start(f32[32,1,128]{2,1,0:T(1,128)} %broadcast_in_dim.15), calls=%async_computation.9 | async-start | bytes 32768 | tf_op jit(solution)/shard_map/all_to_all | solution.py:19
  158.6 20.6 %all-to-all-start.8 = ((f32[32,128,8]{1,2,0:T(8,128)}), f32[32,128,8]{1,2,0:T(8,128)S(1)}, u32[]{:S(2)}, u32[]{:S(2)}) async-start(f32[32,128,8]{1,2,0:T(8,128)} %copy.75), calls=%async_computation.8 | async-start | bytes 262144 | tf_op jit(solution)/shard_map/all_to_all | solution.py:69
  163.1 16.2 %copy-start.12 = (bf16[128,8]{0,1:T(8,128)(2,1)S(1)}, bf16[128,8]{0,1:T(8,128)(2,1)}, u32[]{:S(2)}) copy-start(bf16[128,8]{0,1:T(8,128)(2,1)} %param.16) | copy-start | bytes 6148
  179.9 17.9 %all-to-all-start.10 = ((bf16[32,128,8]{1,2,0:T(8,128)(2,1)}), bf16[32,128,8]{1,2,0:T(8,128)(2,1)S(1)}, u32[]{:S(2)}, u32[]{:S(2)}) async-start(bf16[32,128,8]{1,2,0:T(8,128)(2,1)} %broadcast_in_dim.16), calls=%async_computation.10 | async-start | bytes 131072 | tf_op jit(solution)/shard_map/all_to_all | solution.py:19
  198.8 20.8 %all-to-all-start.11 = ((bf16[16,128,32]{1,2,0:T(8,128)(2,1)}), bf16[16,128,32]{1,2,0:T(8,128)(2,1)S(1)}, u32[]{:S(2)}, u32[]{:S(2)}) async-start(bf16[16,128,32]{1,2,0:T(8,128)(2,1)} %bitcast.22), calls=%async_computation.11 | async-start | bytes 262144 | tf_op jit(solution)/shard_map/all_to_all | solution.py:41
  219.6 4.2 %copy-start.3 = (bf16[512,256]{1,0:T(8,128)(2,1)S(1)}, bf16[512,256]{1,0:T(8,128)(2,1)}, u32[]{:S(2)}) copy-start(bf16[512,256]{1,0:T(8,128)(2,1)} %param.31) | copy-start | bytes 786436
  220.3 10.3 %all-to-all-start.12 = ((bf16[16,128,32]{1,2,0:T(8,128)(2,1)}), bf16[16,128,32]{1,2,0:T(8,128)(2,1)S(1)}, u32[]{:S(2)}, u32[]{:S(2)}) async-start(bf16[16,128,32]{1,2,0:T(8,128)(2,1)} %broadcast_in_dim.17), calls=%async_computation.12 | async-start | bytes 262144 | tf_op jit(solution)/shard_map/all_to_all | solution.py:19
where the time goes:
time: 258 us; the launch traced here: 257 us
  waiting for transfers between devices  87.6 us (34%)
  blocking collectives  76.4 us (30%)
  starting transfers between devices  73.7 us (29%)
  local copies, waits for them, and re-layouts  10.4 us (4%)
  matrix products  5.98 us (2%)
    all_to_all x5, waiting for transfers between devices, from_everyone(): return lax.all_to_all(copies, axis, split_axis=0, concat_axis=0, tiled=True)  47.5 us
    all_to_all x5, starting transfers between devices, from_everyone(): return lax.all_to_all(copies, axis, split_axis=0, concat_axis=0, tiled=True)  36 us
    all_gather x1, blocking collectives, in_one_piece(): whole, at, outs = (lax.all_gather(both, axis, axis=dim, tiled=True), 0, [])  33.5 us
    all_to_all x7, starting transfers between devices, sum_at_owner(): lax.all_to_all(split_up(array, dim, length), axis, 0, 0, tiled=True)  33.3 us
    all_to_all x1, blocking collectives, summed_on_arrival(): lax.all_to_all(split_up(array, dim, length), axis, 0, 0, tiled=True)  25.7 us
    all_to_all x7, waiting for transfers between devices, sum_at_owner(): lax.all_to_all(split_up(array, dim, length), axis, 0, 0, tiled=True)  24 us
    psum x2, blocking collectives, one_axis_at_a_time(): return functools.reduce(lax.psum, axes, array)  17.2 us
    all_to_all x1, waiting for transfers between devices, summed_on_arrival(): lax.all_to_all(split_up(array, dim, length), axis, 0, 0, tiled=True)  16.2 us
  transfers between devices with their start and end apart: 13, of which 11 were waited for; matrix products, arithmetic and copies ran while one was open for 4% of the time, Pallas kernels for 0%

commit v1 on v0

v1 whole, which is shorter than its diff:
```python
import functools
import math

import jax
import jax.numpy as jnp
from jax import lax
from jax.experimental import pallas as pl
from jax.experimental.pallas import tpu as pltpu
from jax.sharding import PartitionSpec as P

EPSILON = 1e-06
F32 = jnp.float32
BF16 = jnp.bfloat16
MESH = pl.DeviceIdType.MESH


def dot(a, b, ca, cb):
    return lax.dot_general(a, b, (((ca,), (cb,)), ((), ())), preferred_element_type=F32)


def kernel(
    nkv,
    ntp,
    width,
    tok_ref,
    gmix_ref,
    wq_ref,
    wk_ref,
    wv_ref,
    wo_ref,
    wgt_ref,
    bias_ref,
    cell_ref,
    norm_ref,
    max_ref,
    ggrp_ref,
    wmix_ref,
    gffn_ref,
    wup_ref,
    wdown_ref,
    out_ref,
    cellnext_ref,
    normnext_ref,
    maxnext_ref,
    tok,
    gmix,
    w4,
    wgt,
    bias,
    cell,
    norm,
    maxs,
    ggrp,
    wmix,
    gffn,
    wup,
    wdown,
    wbig,
    wmixt,
    wupt,
    wdownt,
    cellb,
    ones_tail,
    a_recv,
    b_send,
    b_recv,
    p_send,
    p_recv,
    k_recv,
    c_send,
    c_recv,
    d_send,
    d_recv,
    dsq_send,
    dsq_recv,
    e_send,
    e_recv,
    f_send,
    f_recv,
    fsq_send,
    fsq_recv,
    g_send,
    g_recv,
    h_send,
    h_recv,
    load_sems,
    send_sems,
    recv_sems,
    out_sems,
):
    kv = lax.axis_index("kv")
    tp = lax.axis_index("tp")
    seqs, rows, hd = cell.shape
    heads = norm.shape[1]
    cols, batch = tok.shape
    block = cols * ntp
    share = f_send.shape[1]
    units = share * nkv
    head = tp * rows // hd
    side = tp % 2

    barrier = pltpu.get_barrier_semaphore()

    def greet_tp(i, _):
        pl.semaphore_signal(
            barrier, inc=1, device_id=(kv, lax.rem(tp + i, ntp)), device_id_type=MESH
        )
        return 0

    def greet_kv(i, _):
        pl.semaphore_signal(
            barrier, inc=1, device_id=(lax.rem(kv + i, nkv), tp), device_id_type=MESH
        )
        return 0

    lax.fori_loop(1, ntp, greet_tp, 0)
    lax.fori_loop(1, nkv, greet_kv, 0)

    loads = []
    for i, (src, dst) in enumerate(
        (
            (tok_ref, tok),
            (gmix_ref, gmix),
            (wq_ref, w4.at[0]),
            (wk_ref, w4.at[1]),
            (wv_ref, w4.at[2]),
            (wo_ref, w4.at[3]),
            (wgt_ref, wgt),
            (bias_ref, bias),
            (cell_ref, cell),
            (norm_ref, norm),
            (max_ref, maxs),
            (ggrp_ref, ggrp),
            (wmix_ref, wmix),
            (gffn_ref, gffn),
            (wup_ref, wup),
            (wdown_ref, wdown),
        )
    ):
        copy = pltpu.make_async_copy(src, dst, load_sems.at[i])
        copy.start()
        loads.append(copy)

    def tp_peer(i):
        half = ntp // 2
        return lax.rem(tp + half + (1 - 2 * (i % 2)) * ((i + 1) // 2) + ntp, ntp)

    def kv_peer(i):
        half = nkv // 2
        return lax.rem(kv + half + (1 - 2 * (i % 2)) * ((i + 1) // 2) + nkv, nkv)

    def push(phase, src, dst, device):
        pltpu.make_async_remote_copy(
            src_ref=src,
            dst_ref=dst,
            send_sem=send_sems.at[phase],
            recv_sem=recv_sems.at[phase],
            device_id=device,
            device_id_type=MESH,
        ).start()

    def send_tp(phase, src_of, dst):
        def one(i, _):
            peer = tp_peer(i)
            push(phase, src_of(peer), dst.at[tp], (kv, peer))
            return 0

        lax.fori_loop(0, ntp - 1, one, 0)

    def send_kv(phase, src_of, dst):
        def one(i, _):
            peer = kv_peer(i)
            push(phase, src_of(peer), dst.at[kv], (peer, tp))
            return 0

        lax.fori_loop(0, nkv - 1, one, 0)

    def all_of(phase, buf, count):
        part = buf.at[pl.ds(0, count)]
        return pltpu.make_async_remote_copy(
            src_ref=part,
            dst_ref=part,
            send_sem=send_sems.at[phase],
            recv_sem=recv_sems.at[phase],
            device_id=(kv, lax.rem(tp + 1, ntp)),
            device_id_type=MESH,
        )

    loads[0].wait()
    pl.semaphore_wait(barrier, ntp - 1 + nkv - 1)
    send_tp(0, lambda peer: tok, a_recv)
    a_recv[tp] = tok[...]

    for i in range(1, 16):
        loads[i].wait()
    lane_groups = block // 128 if block >= 128 else 1
    lanes = block // lane_groups
    gpieces = []
    for g in range(lane_groups):
        row = gmix[pl.ds(kv * lane_groups + g, 1), :]
        gpieces.append(jnp.transpose(jnp.broadcast_to(row, (128, lanes))))
    gain_col = jnp.concatenate(gpieces, axis=0)
    for i in range(4):
        wbig[:, i * rows : (i + 1) * rows] = (
            w4[i].astype(F32) * gain_col[:, :rows]
        ).astype(BF16)
    wg = jnp.transpose(wgt[...].astype(F32)) * gain_col[:, : 2 * heads]
    wbig[:, 4 * rows :] = jnp.zeros((block, 128), BF16)
    wbig[:, 4 * rows : 4 * rows + 2 * heads] = wg.astype(BF16)
    lane_id = lax.broadcasted_iota(jnp.int32, (block, 128), 1)
    ones_tail[...] = jnp.where(lane_id < 2 * heads, 0.0, 1.0).astype(BF16)
    grow = ggrp[pl.ds(tp, 1), :]
    wmixt[...] = (jnp.transpose(wmix[...].astype(F32)) * grow).astype(BF16)
    frow = jnp.concatenate(
        [gffn[pl.ds(kv * lane_groups + g, 1), :] for g in range(lane_groups)], axis=1
    )
    wupt[...] = (jnp.transpose(wup[...].astype(F32)) * frow).astype(BF16)
    wdownt[...] = jnp.transpose(wdown[...].astype(F32)).astype(BF16)
    for s in range(seqs):
        cellb[s] = cell[s].astype(BF16)
    head_of = lax.broadcasted_iota(jnp.int32, (seqs, heads, hd), 1)
    norm_own = jnp.sum(jnp.where(head_of == head, norm[...], 0.0), axis=1)

    all_of(0, a_recv, ntp - 1).wait_recv()
    xf = a_recv[...].astype(F32).reshape(block, batch)
    xb = xf.astype(BF16)
    xsq = (xf * xf).astype(BF16)
    part = dot(xb, wbig[...], 0, 0)
    tail = dot(xsq, ones_tail[...], 0, 0)
    b_send[:, :, : 4 * rows] = part[:, : 4 * rows].reshape(nkv, seqs, 4 * rows).astype(BF16)
    b_send[:, :, 4 * rows :] = (
        (part[:, 4 * rows :] + tail).reshape(nkv, seqs, 128).astype(BF16)
    )
    send_kv(1, lambda peer: b_send.at[peer], b_recv)
    b_recv[kv] = b_send[kv]
    all_of(1, b_recv, nkv - 1).wait_recv()
    total = b_recv[0].astype(F32)
    for j in range(1, nkv):
        total = total + b_recv[j].astype(F32)
    scale_in = lax.rsqrt(
        total[:, 4 * rows + 2 * heads : 4 * rows + 2 * heads + 1] / width + EPSILON
    )
    total = total * scale_in
    q_part = total[:, :rows].astype(BF16)
    k_part = total[:, rows : 2 * rows].astype(BF16)
    values = total[:, 2 * rows : 3 * rows]
    gate_out = total[:, 3 * rows : 4 * rows]
    gate_in = total[:, 4 * rows : 4 * rows + heads]
    gate_forget = total[:, 4 * rows + heads : 4 * rows + 2 * heads]

    p_send[0] = q_part
    p_send[1] = k_part
    sibling = tp + 1 - 2 * side
    pair = pltpu.make_async_remote_copy(
        src_ref=p_send,
        dst_ref=p_recv,
        send_sem=send_sems.at[2],
        recv_sem=recv_sems.at[2],
        device_id=(kv, sibling),
        device_id_type=MESH,
    )
    pair.start()

    arg = gate_forget + bias[...]
    log_forget = jnp.minimum(arg, 0.0) - jnp.log1p(jnp.exp(-jnp.abs(arg)))
    carried = log_forget + maxs[...]
    max_next = jnp.maximum(carried, gate_in)
    decay = jnp.exp(carried - max_next)
    inflow = jnp.exp(gate_in - max_next)
    maxnext_ref[...] = max_next
    head_lane = lax.broadcasted_iota(jnp.int32, (seqs, heads), 1)
    dec = jnp.sum(jnp.where(head_lane == head, decay, 0.0), axis=1, keepdims=True)
    inf = jnp.sum(jnp.where(head_lane == head, inflow, 0.0), axis=1, keepdims=True)
    gate_sig = jax.nn.sigmoid(gate_out)

    pair.wait_recv()
    q_other = p_recv[0].astype(F32)
    k_other = p_recv[1].astype(F32)
    q_mine = q_part.astype(F32)
    k_mine = k_part.astype(F32)
    first = side == 0
    qf = jnp.concatenate(
        [jnp.where(first, q_mine, q_other), jnp.where(first, q_other, q_mine)], axis=1
    )
    kf = jnp.concatenate(
        [jnp.where(first, k_mine, k_other), jnp.where(first, k_other, k_mine)], axis=1
    ) / math.sqrt(hd)
    kq = jnp.sum(kf * qf, axis=1, keepdims=True)
    nq = jnp.sum(norm_own * qf, axis=1, keepdims=True)
    denom = jnp.maximum(jnp.abs(dec * nq + inf * kq), 1.0)
    row_id = lax.broadcasted_iota(jnp.int32, (seqs, hd), 0)
    cq = jnp.zeros((seqs, rows), F32)
    for s in range(seqs):
        cq = cq + dot(jnp.where(row_id == s, qf, 0.0).astype(BF16), cellb[s], 1, 1)
    iv = inf * values
    read = gate_sig * ((dec * cq + iv * kq) / denom)

    c_send[...] = read.astype(BF16)
    send_kv(3, lambda peer: c_send, c_recv)
    c_recv[kv] = c_send[...]
    send_tp(4, lambda peer: p_send.at[1], k_recv)
    k_recv[tp] = p_send[1]
    ivt = jnp.transpose(iv)
    for s in range(seqs):
        cell[s] = dec[s : s + 1, :] * cell[s] + ivt[:, s : s + 1] * kf[s : s + 1, :]
    cell_out = pltpu.make_async_copy(cell, cellnext_ref, out_sems.at[0])
    cell_out.start()

    all_of(3, c_recv, nkv - 1).wait_recv()
    rf = c_recv[...].astype(F32).reshape(batch, rows)
    rb = rf.astype(BF16)
    sq = dot(jnp.ones((8, rows), BF16), (rf * rf).astype(BF16), 1, 1)
    dsq_send[...] = sq[0:1, :]
    mixt = dot(wmixt[...], rb, 1, 1)
    d_send[...] = mixt.reshape(ntp, cols, batch).astype(BF16)
    send_tp(5, lambda peer: d_send.at[peer], d_recv)
    send_tp(6, lambda peer: dsq_send, dsq_recv)
    d_recv[tp] = d_send[tp]
    dsq_recv[tp] = dsq_send[...]
    all_of(5, d_recv, ntp - 1).wait_recv()
    all_of(6, dsq_recv, ntp - 1).wait_recv()
    mix_sum = d_recv[0].astype(F32)
    sq_sum = dsq_recv[0]
    for j in range(1, ntp):
        mix_sum = mix_sum + d_recv[j].astype(F32)
        sq_sum = sq_sum + dsq_recv[j]
    scale_group = lax.rsqrt(sq_sum / (heads * hd) + EPSILON)
    mixed = (tok[...].astype(F32) + mix_sum * scale_group).astype(BF16)

    e_send[...] = mixed
    send_tp(7, lambda peer: e_send, e_recv)
    e_recv[tp] = e_send[...]
    all_of(7, e_recv, ntp - 1).wait_recv()
    mf = e_recv[...].astype(F32).reshape(block, batch)
    fsq_send[...] = jnp.sum(mf * mf, axis=0, keepdims=True)
    send_kv(8, lambda peer: fsq_send, fsq_recv)
    fsq_recv[kv] = fsq_send[...]
    upt = dot(wupt[...], mf.astype(BF16), 1, 0)
    f_send[...] = upt.reshape(nkv, share, batch).astype(BF16)
    send_kv(9, lambda peer: f_send.at[peer], f_recv)
    f_recv[kv] = f_send[kv]
    all_of(8, fsq_recv, nkv - 1).wait_recv()
    fsq_sum = fsq_recv[0]
    for j in range(1, nkv):
        fsq_sum = fsq_sum + fsq_recv[j]
    scale_ffn = lax.rsqrt(fsq_sum / width + EPSILON)
    all_of(9, f_recv, nkv - 1).wait_recv()
    up = f_recv[0].astype(F32)
    for j in range(1, nkv):
        up = up + f_recv[j].astype(F32)
    hid = jnp.maximum(up * scale_ffn, 0.0)

    g_send[...] = (hid * hid).astype(BF16)
    send_kv(10, lambda peer: g_send, g_recv)
    g_recv[kv] = g_send[...]
    all_of(4, k_recv, ntp - 1).wait_recv()
    per_head = hd // rows
    for h in range(heads):
        key = jnp.concatenate(
            [k_recv[h * per_head + i].astype(F32) for i in range(per_head)], axis=1
        ) / math.sqrt(hd)
        norm[:, h, :] = decay[:, h : h + 1] * norm[:, h, :] + inflow[:, h : h + 1] * key
    norm_out = pltpu.make_async_copy(norm, normnext_ref, out_sems.at[1])
    norm_out.start()

    all_of(10, g_recv, nkv - 1).wait_recv()
    hidden = g_recv[...].reshape(units, batch)
    downt = dot(wdownt[...], hidden, 1, 0)
    h_send[...] = downt.reshape(ntp, cols, batch).astype(BF16)
    send_tp(11, lambda peer: h_send.at[peer], h_recv)
    h_recv[tp] = h_send[tp]

    all_of(0, a_recv, ntp - 1).wait_send()
    all_of(1, b_recv, nkv - 1).wait_send()
    pair.wait_send()
    all_of(3, c_recv, nkv - 1).wait_send()
    all_of(4, k_recv, ntp - 1).wait_send()
    all_of(5, d_recv, ntp - 1).wait_send()
    all_of(6, dsq_recv, ntp - 1).wait_send()
    all_of(7, e_recv, ntp - 1).wait_send()
    all_of(8, fsq_recv, nkv - 1).wait_send()
    all_of(9, f_recv, nkv - 1).wait_send()
    all_of(10, g_recv, nkv - 1).wait_send()
    cell_out.wait()
    norm_out.wait()

    all_of(11, h_recv, ntp - 1).wait_recv()
    down = h_recv[0].astype(F32)
    for j in range(1, ntp):
        down = down + h_recv[j].astype(F32)
    out_ref[...] = (mixed.astype(F32) + down).astype(BF16)
    all_of(11, h_recv, ntp - 1).wait_send()


def per_device(nkv, ntp, *args):
    (
        tokens,
        gain_mix,
        w_query,
        w_key,
        w_value,
        w_outgate,
        w_gates,
        forget_bias,
        cell_state,
        norm_state,
        max_state,
        gain_group,
        w_mix,
        gain_ffn,
        w_up,
        w_down,
    ) = args
    batch, cols = tokens.shape
    width = gain_mix.shape[0]
    seqs, rows, hd = cell_state.shape
    heads = forget_bias.shape[0]
    block = w_query.shape[0]
    units = w_up.shape[1]
    share = units // nkv
    lanes = min(block, 128)
    operands = (
        tokens.T,
        gain_mix.reshape(-1, lanes),
        w_query,
        w_key,
        w_value,
        w_outgate,
        w_gates.T,
        forget_bias.reshape(1, heads),
        cell_state,
        norm_state,
        max_state,
        gain_group.reshape(-1, rows),
        w_mix,
        gain_ffn.reshape(-1, lanes),
        w_up,
        w_down,
    )
    wide = 4 * rows + 128
    vmem = pltpu.VMEM
    scratch = [
        vmem((cols, batch), BF16),
        vmem((width // lanes, lanes), F32),
        vmem((4, block, rows), BF16),
        vmem((2 * heads, block), BF16),
        vmem((1, heads), F32),
        vmem((seqs, rows, hd), F32),
        vmem((seqs, heads, hd), F32),
        vmem((seqs, heads), F32),
        vmem((heads * hd // rows, rows), F32),
        vmem((rows, block), BF16),
        vmem((width // lanes, lanes), F32),
        vmem((block, units), BF16),
        vmem((units, block), BF16),
        vmem((block, wide), BF16),
        vmem((block, rows), BF16),
        vmem((units, block), BF16),
        vmem((block, units), BF16),
        vmem((seqs, rows, hd), BF16),
        vmem((block, 128), BF16),
        vmem((ntp, cols, batch), BF16),
        vmem((nkv, seqs, wide), BF16),
        vmem((nkv, seqs, wide), BF16),
        vmem((2, seqs, rows), BF16),
        vmem((2, seqs, rows), BF16),
        vmem((ntp, seqs, rows), BF16),
        vmem((seqs, rows), BF16),
        vmem((nkv, seqs, rows), BF16),
        vmem((ntp, cols, batch), BF16),
        vmem((ntp, cols, batch), BF16),
        vmem((1, batch), F32),
        vmem((ntp, 1, batch), F32),
        vmem((cols, batch), BF16),
        vmem((ntp, cols, batch), BF16),
        vmem((nkv, share, batch), BF16),
        vmem((nkv, share, batch), BF16),
        vmem((1, batch), F32),
        vmem((nkv, 1, batch), F32),
        vmem((share, batch), BF16),
        vmem((nkv, share, batch), BF16),
        vmem((ntp, cols, batch), BF16),
        vmem((ntp, cols, batch), BF16),
        pltpu.SemaphoreType.DMA((16,)),
        pltpu.SemaphoreType.DMA((12,)),
        pltpu.SemaphoreType.DMA((12,)),
        pltpu.SemaphoreType.DMA((2,)),
    ]
    anywhere = pl.BlockSpec(memory_space=pl.ANY)
    in_vmem = pl.BlockSpec(memory_space=pltpu.VMEM)
    out, cell_next, norm_next, max_next = pl.pallas_call(
        functools.partial(kernel, nkv, ntp, width),
        out_shape=(
            jax.ShapeDtypeStruct((cols, batch), BF16),
            jax.ShapeDtypeStruct(cell_state.shape, F32),
            jax.ShapeDtypeStruct(norm_state.shape, F32),
            jax.ShapeDtypeStruct(max_state.shape, F32),
        ),
        in_specs=[anywhere] * len(operands),
        out_specs=(in_vmem, anywhere, anywhere, in_vmem),
        scratch_shapes=scratch,
        compiler_params=pltpu.CompilerParams(collective_id=0, has_side_effects=True),
        name="decode_step",
    )(*operands)
    return out.T, cell_next, norm_next, max_next


def solution(mesh):
    kv_tp = ("kv", "tp")
    in_specs = (
        P(None, kv_tp),
        P(),
        P("kv", "tp"),
        P("kv", "tp"),
        P("kv", "tp"),
        P("kv", "tp"),
        P("kv", None),
        P(),
        P("kv", "tp", None),
        P("kv", None, None),
        P("kv", None),
        P(),
        P("tp", "kv"),
        P(),
        P("kv", "tp"),
        P("tp", "kv"),
    )
    out_specs = (P(None, kv_tp), P("kv", "tp", None), P("kv", None, None), P("kv", None))
    body = functools.partial(per_device, mesh.shape["kv"], mesh.shape["tp"])
    return jax.shard_map(
        body, mesh=mesh, in_specs=in_specs, out_specs=out_specs, check_vma=False
    )
```

time: 258 us -> 78.6 us (0.30)
  waiting for transfers between devices: 87.6 us -> 0 us
  blocking collectives: 76.4 us -> 0 us
  starting transfers between devices: 73.7 us -> 0 us
  Pallas kernels: 0 us -> 72.9 us
  matrix products: 5.98 us -> 0 us
  local copies, waits for them, and re-layouts: 10.4 us -> 4.83 us
    all_to_all x13 -> x0, waiting for transfers between devices: 87.6 us -> none  [the longest x5 47.5 us: from_everyone(): return lax.all_to_all(copies, axis, split_axis=0, concat_axis=0, tiled=True)]
    all_to_all x13 -> x0, starting transfers between devices: 73.7 us -> none  [the longest x5 36 us: from_everyone(): return lax.all_to_all(copies, axis, split_axis=0, concat_axis=0, tiled=True)]
    pallas_call x0 -> x1, Pallas kernels: none -> 72.9 us  [per_device(): pl.pallas_call(functools.partial(kernel, nkv, ntp, width), out_shape=(jax...]
    all_gather x1 -> x0, blocking collectives: 33.5 us -> none  [in_one_piece(): whole, at, outs = (lax.all_gather(both, axis, axis=dim, tiled=True), 0, [])]
    all_to_all x1 -> x0, blocking collectives: 25.7 us -> none  [summed_on_arrival(): lax.all_to_all(split_up(array, dim, length), axis, 0, 0, tiled=True)]
    psum x2 -> x0, blocking collectives: 17.2 us -> none  [one_axis_at_a_time(): return functools.reduce(lax.psum, axes, array)]
    dot_general x13 -> x0, matrix products: 5.98 us -> none  [the longest x5 3.79 us: per_device(): jnp.dot(normed, weight, preferred_element_type=f32)]
    broadcast_in_dim x6 -> x0, local copies, waits for them, and re-layouts: 3.98 us -> none  [from_everyone(): copies = jnp.broadcast_to(array, (lax.axis_size(axis), *array.shape))]
  transfers between devices with their start and end apart: 13 -> 0, of which waited for: 11 -> 0; matrix products, arithmetic and copies ran while one was open for 4% -> 0% of each run, Pallas kernels for 0% -> 0%
where the time goes in v1:
time: 78.6 us; the launch traced here: 78.4 us
  Pallas kernels  72.9 us (93%)
  local copies, waits for them, and re-layouts  4.83 us (6%)
    pallas_call x1, Pallas kernels, per_device(): pl.pallas_call(functools.partial(kernel, nkv, ntp, width), out_shape=(jax...  72.9 us
    unnamed x10, local copies, waits for them, and re-layouts  4.83 us

profile of v1, /device:TPU:1, one launch (start us, length us, event | category | flops | bytes accessed | tf_op | source)
XLA Modules:
  0.0 78.4 jit_solution(7137280846026166107)
XLA Ops:
  0.6 72.9 %decode_step.1 = (bf16[8,128]{1,0:T(8,128)(2,1)}, f32[8,128,256]{2,1,0:T(8,128)}, f32[8,16,256]{2,1,0:T(8,128)}, f32[8,16]{1,0:T(8,128)}) custom-call(bf16[8,128]{1,0:T(8,128)(2,1)} %bitcast.12, f32[32,128]{1,0:T(8,128)} %bitcast.7, bf16[256,128]{1,0:T(8,128)(2,1)} %wq_ref.1, bf16[256,128]{1,0:T(8,128)(2,1)} %wk_ref.1, bf16[256,128]{1,0:T(8,128)(2,1)} %wv_ref.1, ...), custom_call_target="tpu_custom_call" | custom-call | tf_op jit(solution)/shard_map/decode_step/pallas_call | solution.py:491
  73.5 0.0 copy-start.2
  73.5 0.7 copy-done.2
  74.2 0.6 copy.24
  74.8 0.0 copy-start
  74.8 2.3 %copy.25 = f32[8,128,256]{2,1,0:T(8,128)} copy(f32[8,128,256]{2,1,0:T(8,128)} %get-tuple-element.17) | data formatting | bytes 2097152
  77.1 0.0 copy-done
  77.1 0.0 copy-start.1
  77.1 0.7 copy.26
  77.7 0.0 copy-done.1
  77.8 0.6 copy.27
Async XLA Ops:
  73.5 0.7 copy-start.2
  74.8 2.3 %copy-start = (f32[8,16,256]{2,1,0:T(8,128)S(1)}, f32[8,16,256]{2,1,0:T(8,128)}, u32[]{:S(2)}) copy-start(f32[8,16,256]{2,1,0:T(8,128)} %get-tuple-element.18) | copy-start | bytes 393220
  77.1 0.7 copy-start.1

commit v2 on v1

v2 whole, which is shorter than its diff:
```python
import functools
import math

import jax
import jax.numpy as jnp
from jax import lax
from jax.experimental import pallas as pl
from jax.experimental.pallas import tpu as pltpu
from jax.sharding import PartitionSpec as P

EPSILON = 1e-06
F32 = jnp.float32
BF16 = jnp.bfloat16
MESH = pl.DeviceIdType.MESH


def dot(a, b, ca, cb):
    return lax.dot_general(a, b, (((ca,), (cb,)), ((), ())), preferred_element_type=F32)


def two_parts(total):
    high = total.astype(BF16)
    return jnp.concatenate([high, (total - high.astype(F32)).astype(BF16)], axis=0)


def kernel(
    nkv,
    ntp,
    width,
    tok_ref,
    gmix_ref,
    wq_ref,
    wk_ref,
    wv_ref,
    wo_ref,
    wgt_ref,
    bias_ref,
    cell_ref,
    norm_ref,
    max_ref,
    ggrp_ref,
    wmix_ref,
    gffn_ref,
    wup_ref,
    wdown_ref,
    out_ref,
    cellnext_ref,
    normnext_ref,
    maxnext_ref,
    tok,
    gmix,
    w4,
    wgt,
    bias,
    maxs,
    ggrp,
    wmix,
    gffn,
    wup,
    wdown,
    wqk_other,
    wbig,
    wmixt,
    wupt,
    wdownt,
    cellb,
    ones_tail,
    a_recv,
    b_send,
    b_recv,
    k_send,
    k_recv,
    c_send,
    c_recv,
    d_send,
    d_recv,
    e_send,
    e_recv,
    f_send,
    f_recv,
    g_send,
    g_recv,
    h_send,
    h_recv,
    load_sems,
    send_sems,
    recv_sems,
):
    kv = lax.axis_index("kv")
    tp = lax.axis_index("tp")
    cell, norm = cellnext_ref, normnext_ref
    seqs, rows, hd = cell.shape
    heads = norm.shape[1]
    cols, batch = tok.shape
    block = cols * ntp
    share = g_send.shape[0]
    units = share * nkv
    head = tp * rows // hd
    side = tp % 2
    sibling = tp + 1 - 2 * side
    first = side == 0
    reach = ntp // 8

    loads = []
    for i, (src, dst) in enumerate(
        (
            (tok_ref, tok),
            (wq_ref, w4.at[0]),
            (wk_ref, w4.at[1]),
            (gmix_ref, gmix),
            (wv_ref, w4.at[2]),
            (wo_ref, w4.at[3]),
            (wgt_ref, wgt),
            (bias_ref, bias),
            (cell_ref, cell),
            (norm_ref, norm),
            (max_ref, maxs),
            (ggrp_ref, ggrp),
            (wmix_ref, wmix),
            (gffn_ref, gffn),
            (wup_ref, wup),
            (wdown_ref, wdown),
        )
    ):
        loads.append(pltpu.make_async_copy(src, dst, load_sems.at[i]))
    loads[0].start()

    barrier = pltpu.get_barrier_semaphore()

    def near(i):
        chips = reach - i // 4
        return lax.rem(tp + 2 * chips * (1 - 2 * (i % 2)) + (i // 2) % 2 + ntp - side, ntp)

    def greet_tp(i, _):
        pl.semaphore_signal(barrier, inc=1, device_id=(kv, near(i)), device_id_type=MESH)
        return 0

    def greet_kv(i, _):
        pl.semaphore_signal(barrier, inc=1, device_id=(kv_peer(i), tp), device_id_type=MESH)
        return 0

    def tp_peer(i):
        half = ntp // 2
        return lax.rem(tp + half + (1 - 2 * (i % 2)) * ((i + 1) // 2) + ntp, ntp)

    def kv_peer(i):
        half = nkv // 2
        return lax.rem(kv + half + (1 - 2 * (i % 2)) * ((i + 1) // 2) + nkv, nkv)

    lax.fori_loop(0, 4 * reach, greet_tp, 0)
    lax.fori_loop(0, nkv - 1, greet_kv, 0)
    pl.semaphore_signal(barrier, inc=1, device_id=(kv, sibling), device_id_type=MESH)
    for copy in loads[1:]:
        copy.start()

    def push(phase, src, dst, device):
        pltpu.make_async_remote_copy(
            src_ref=src,
            dst_ref=dst,
            send_sem=send_sems.at[phase],
            recv_sem=recv_sems.at[phase],
            device_id=device,
            device_id_type=MESH,
        ).start()

    def send_tp(phase, src_of, dst):
        def one(i, _):
            peer = tp_peer(i)
            push(phase, src_of(peer), dst.at[tp], (kv, peer))
            return 0

        lax.fori_loop(0, ntp - 1, one, 0)

    def send_kv(phase, src_of, dst):
        def one(i, _):
            peer = kv_peer(i)
            push(phase, src_of(peer), dst.at[kv], (peer, tp))
            return 0

        lax.fori_loop(0, nkv - 1, one, 0)

    def all_of(phase, buf, count):
        part = buf.at[pl.ds(0, count)]
        return pltpu.make_async_remote_copy(
            src_ref=part,
            dst_ref=part,
            send_sem=send_sems.at[phase],
            recv_sem=recv_sems.at[phase],
            device_id=(kv, lax.rem(tp + 1, ntp)),
            device_id_type=MESH,
        )

    def send_near(i, _):
        down = i % 2
        pltpu.make_async_remote_copy(
            src_ref=tok,
            dst_ref=a_recv.at[tp],
            send_sem=send_sems.at[0],
            recv_sem=recv_sems.at[12 + down],
            device_id=(kv, near(i)),
            device_id_type=MESH,
        ).start()
        return 0

    def hand_on(phase, chip, steps, to):
        def one(i, _):
            at = 2 * lax.rem(chip + i + ntp // 2, ntp // 2)
            pair = a_recv.at[pl.ds(at, 2)]
            push(phase, pair, pair, (kv, lax.rem(tp + 2 * to + ntp, ntp)))
            return 0

        lax.fori_loop(0, steps, one, 0)

    loads[0].wait()
    pl.semaphore_wait(barrier, 4 * reach + nkv)
    lax.fori_loop(0, 4 * reach, send_near, 0)
    push(2, tok, a_recv.at[tp], (kv, sibling))
    loads[1].wait()
    loads[2].wait()
    push(3, w4.at[pl.ds(0, 2)], wqk_other, (kv, sibling))
    a_recv[tp] = tok[...]
    chip = tp // 2
    all_of(12, a_recv, 2 * reach).wait_recv()
    if reach > 1:
        hand_on(0, chip - reach + 1, reach - 1, reach)
    all_of(13, a_recv, 2 * reach).wait_recv()
    hand_on(0, chip + 1, reach, -reach)

    for i in range(3, 16):
        loads[i].wait()
    lane_groups = block // 128 if block >= 128 else 1
    lanes = block // lane_groups
    gpieces = []
    for g in range(lane_groups):
        row = gmix[pl.ds(kv * lane_groups + g, 1), :]
        gpieces.append(jnp.transpose(jnp.broadcast_to(row, (128, lanes))))
    gain_col = jnp.concatenate(gpieces, axis=0)
    gain = gain_col[:, :rows]
    wbig[:, 2 * hd : 2 * hd + rows] = (w4[2].astype(F32) * gain).astype(BF16)
    wbig[:, 2 * hd + rows : 2 * hd + 2 * rows] = (w4[3].astype(F32) * gain).astype(BF16)
    wg = jnp.transpose(wgt[...].astype(F32)) * gain_col[:, : 2 * heads]
    tail_at = 2 * hd + 2 * rows
    wbig[:, tail_at:] = jnp.zeros((block, 128), BF16)
    wbig[:, tail_at : tail_at + 2 * heads] = wg.astype(BF16)
    lane_id = lax.broadcasted_iota(jnp.int32, (block, 128), 1)
    ones_tail[...] = jnp.where(lane_id < 2 * heads, 0.0, 1.0).astype(BF16)
    grow = ggrp[pl.ds(tp, 1), :]
    wmixt[...] = (jnp.transpose(wmix[...].astype(F32)) * grow).astype(BF16)
    frow = jnp.concatenate(
        [gffn[pl.ds(kv * lane_groups + g, 1), :] for g in range(lane_groups)], axis=1
    )
    wupt[...] = (jnp.transpose(wup[...].astype(F32)) * frow).astype(BF16)
    wdownt[...] = jnp.transpose(wdown[...].astype(F32)).astype(BF16)
    for s in range(seqs):
        cellb[s] = cell[s].astype(BF16)
    head_of = lax.broadcasted_iota(jnp.int32, (seqs, heads, hd), 1)
    norm_own = jnp.sum(jnp.where(head_of == head, norm[...], 0.0), axis=1)

    pltpu.make_async_remote_copy(
        src_ref=wqk_other,
        dst_ref=wqk_other,
        send_sem=send_sems.at[3],
        recv_sem=recv_sems.at[3],
        device_id=(kv, sibling),
        device_id_type=MESH,
    ).wait_recv()
    for i in range(2):
        mine = w4[i].astype(F32)
        other = wqk_other[i].astype(F32)
        low = jnp.where(first, mine, other)
        high = jnp.where(first, other, mine)
        wbig[:, i * hd : i * hd + rows] = (low * gain).astype(BF16)
        wbig[:, i * hd + rows : (i + 1) * hd] = (high * gain).astype(BF16)

    all_of(2, a_recv, 1).wait_recv()
    all_of(0, a_recv, ntp - 2 - 4 * reach).wait_recv()
    xf = a_recv[...].astype(F32).reshape(block, batch)
    xb = xf.astype(BF16)
    xsq = (xf * xf).astype(BF16)
    part = dot(xb, wbig[...], 0, 0)
    tail = dot(xsq, ones_tail[...], 0, 0)
    b_send[:, :, :tail_at] = part[:, :tail_at].reshape(nkv, seqs, tail_at).astype(BF16)
    b_send[:, :, tail_at:] = (part[:, tail_at:] + tail).reshape(nkv, seqs, 128).astype(BF16)
    send_kv(1, lambda peer: b_send.at[peer], b_recv)
    b_recv[kv] = b_send[kv]
    all_of(1, b_recv, nkv - 1).wait_recv()
    total = b_recv[0].astype(F32)
    for j in range(1, nkv):
        total = total + b_recv[j].astype(F32)
    ends = tail_at + 2 * heads
    scale_in = lax.rsqrt(total[:, ends : ends + 1] / width + EPSILON)
    total = total * scale_in
    qf = total[:, :hd].astype(BF16).astype(F32)
    keys = total[:, hd : 2 * hd].astype(BF16)
    kf = keys.astype(F32) / math.sqrt(hd)
    values = total[:, 2 * hd : 2 * hd + rows]
    gate_out = total[:, 2 * hd + rows : tail_at]
    gate_in = total[:, tail_at : tail_at + heads]
    gate_forget = total[:, tail_at + heads : ends]

    arg = gate_forget + bias[...]
    log_forget = jnp.minimum(arg, 0.0) - jnp.log1p(jnp.exp(-jnp.abs(arg)))
    carried = log_forget + maxs[...]
    max_next = jnp.maximum(carried, gate_in)
    decay = jnp.exp(carried - max_next)
    inflow = jnp.exp(gate_in - max_next)
    maxnext_ref[...] = max_next
    head_lane = lax.broadcasted_iota(jnp.int32, (seqs, heads), 1)
    dec = jnp.sum(jnp.where(head_lane == head, decay, 0.0), axis=1, keepdims=True)
    inf = jnp.sum(jnp.where(head_lane == head, inflow, 0.0), axis=1, keepdims=True)
    gate_sig = jax.nn.sigmoid(gate_out)

    kq = jnp.sum(kf * qf, axis=1, keepdims=True)
    nq = jnp.sum(norm_own * qf, axis=1, keepdims=True)
    denom = jnp.maximum(jnp.abs(dec * nq + inf * kq), 1.0)
    row_id = lax.broadcasted_iota(jnp.int32, (seqs, hd), 0)
    cq = jnp.zeros((seqs, rows), F32)
    for s in range(seqs):
        cq = cq + dot(jnp.where(row_id == s, qf, 0.0).astype(BF16), cellb[s], 1, 1)
    iv = inf * values
    read = gate_sig * ((dec * cq + iv * kq) / denom)

    c_send[...] = read.astype(BF16)
    send_kv(6, lambda peer: c_send, c_recv)
    c_recv[kv] = c_send[...]
    k_send[...] = keys

    def send_keys(i, _):
        half = ntp // 4
        away = half + (1 - 2 * (i % 2)) * ((i + 1) // 2)
        push(4, k_send, k_recv.at[chip], (kv, lax.rem(tp + 2 * away + ntp, ntp)))
        return 0

    lax.fori_loop(0, ntp // 2 - 1, send_keys, 0)
    k_recv[chip] = k_send[...]
    ivt = jnp.transpose(iv)
    for s in range(seqs):
        cell[s] = dec[s : s + 1, :] * cell[s] + ivt[:, s : s + 1] * kf[s : s + 1, :]

    all_of(6, c_recv, nkv - 1).wait_recv()
    rf = c_recv[...].astype(F32).reshape(batch, rows)
    rb = rf.astype(BF16)
    sq = dot(jnp.ones((8, rows), BF16), (rf * rf).astype(BF16), 1, 1)
    d_send[:, cols:, :] = jnp.broadcast_to(two_parts(sq[0:1, :])[None], (ntp, 2, batch))
    mixt = dot(wmixt[...], rb, 1, 1)
    d_send[:, :cols, :] = mixt.reshape(ntp, cols, batch).astype(BF16)
    send_tp(5, lambda peer: d_send.at[peer], d_recv)
    d_recv[tp] = d_send[tp]
    all_of(5, d_recv, ntp - 1).wait_recv()
    both = d_recv[0].astype(F32)
    for j in range(1, ntp):
        both = both + d_recv[j].astype(F32)
    mix_sum = both[:cols]
    sq_sum = both[cols : cols + 1] + both[cols + 1 : cols + 2]
    scale_group = lax.rsqrt(sq_sum / (heads * hd) + EPSILON)
    mixed = (tok[...].astype(F32) + mix_sum * scale_group).astype(BF16)

    e_send[...] = mixed
    send_tp(7, lambda peer: e_send, e_recv)
    e_recv[tp] = e_send[...]
    all_of(7, e_recv, ntp - 1).wait_recv()
    mf = e_recv[...].astype(F32).reshape(block, batch)
    upt = dot(wupt[...], mf.astype(BF16), 1, 0)
    fsq = two_parts(jnp.sum(mf * mf, axis=0, keepdims=True))
    f_send[:, share:, :] = jnp.broadcast_to(fsq[None], (nkv, 2, batch))
    f_send[:, :share, :] = upt.reshape(nkv, share, batch).astype(BF16)
    send_kv(9, lambda peer: f_send.at[peer], f_recv)
    f_recv[kv] = f_send[kv]
    all_of(9, f_recv, nkv - 1).wait_recv()
    both = f_recv[0].astype(F32)
    for j in range(1, nkv):
        both = both + f_recv[j].astype(F32)
    up = both[:share]
    fsq_sum = both[share : share + 1] + both[share + 1 : share + 2]
    scale_ffn = lax.rsqrt(fsq_sum / width + EPSILON)
    hid = jnp.maximum(up * scale_ffn, 0.0)

    g_send[...] = (hid * hid).astype(BF16)
    send_kv(10, lambda peer: g_send, g_recv)
    g_recv[kv] = g_send[...]
    all_of(4, k_recv, ntp // 2 - 1).wait_recv()
    for h in range(heads):
        key = k_recv[h].astype(F32) / math.sqrt(hd)
        norm[:, h, :] = decay[:, h : h + 1] * norm[:, h, :] + inflow[:, h : h + 1] * key

    all_of(10, g_recv, nkv - 1).wait_recv()
    hidden = g_recv[...].reshape(units, batch)
    downt = dot(wdownt[...], hidden, 1, 0)
    h_send[...] = downt.reshape(ntp, cols, batch).astype(BF16)
    send_tp(11, lambda peer: h_send.at[peer], h_recv)
    h_recv[tp] = h_send[tp]

    all_of(0, a_recv, ntp - 2).wait_send()
    all_of(2, a_recv, 1).wait_send()
    pltpu.make_async_remote_copy(
        src_ref=wqk_other,
        dst_ref=wqk_other,
        send_sem=send_sems.at[3],
        recv_sem=recv_sems.at[3],
        device_id=(kv, sibling),
        device_id_type=MESH,
    ).wait_send()
    all_of(1, b_recv, nkv - 1).wait_send()
    all_of(6, c_recv, nkv - 1).wait_send()
    all_of(4, k_recv, ntp // 2 - 1).wait_send()
    all_of(5, d_recv, ntp - 1).wait_send()
    all_of(7, e_recv, ntp - 1).wait_send()
    all_of(9, f_recv, nkv - 1).wait_send()
    all_of(10, g_recv, nkv - 1).wait_send()

    all_of(11, h_recv, ntp - 1).wait_recv()
    down = h_recv[0].astype(F32)
    for j in range(1, ntp):
        down = down + h_recv[j].astype(F32)
    out_ref[...] = (mixed.astype(F32) + down).astype(BF16)
    all_of(11, h_recv, ntp - 1).wait_send()


def write_out(*refs):
    sems = refs[8]
    copies = [pltpu.make_async_copy(refs[i], refs[4 + i], sems.at[i]) for i in range(4)]
    for i in (1, 2, 3, 0):
        copies[i].start()
    for copy in copies:
        copy.wait()


def per_device(nkv, ntp, *args):
    (
        tokens,
        gain_mix,
        w_query,
        w_key,
        w_value,
        w_outgate,
        w_gates,
        forget_bias,
        cell_state,
        norm_state,
        max_state,
        gain_group,
        w_mix,
        gain_ffn,
        w_up,
        w_down,
    ) = args
    batch, cols = tokens.shape
    width = gain_mix.shape[0]
    seqs, rows, hd = cell_state.shape
    heads = forget_bias.shape[0]
    block = w_query.shape[0]
    units = w_up.shape[1]
    share = units // nkv
    lanes = min(block, 128)
    operands = (
        tokens.T,
        gain_mix.reshape(-1, lanes),
        w_query,
        w_key,
        w_value,
        w_outgate,
        w_gates.T,
        forget_bias.reshape(1, heads),
        cell_state,
        norm_state,
        max_state,
        gain_group.reshape(-1, rows),
        w_mix,
        gain_ffn.reshape(-1, lanes),
        w_up,
        w_down,
    )
    wide = 2 * hd + 2 * rows + 128
    vmem = pltpu.VMEM
    scratch = [
        vmem((cols, batch), BF16),
        vmem((width // lanes, lanes), F32),
        vmem((4, block, rows), BF16),
        vmem((2 * heads, block), BF16),
        vmem((1, heads), F32),
        vmem((seqs, heads), F32),
        vmem((heads * hd // rows, rows), F32),
        vmem((rows, block), BF16),
        vmem((width // lanes, lanes), F32),
        vmem((block, units), BF16),
        vmem((units, block), BF16),
        vmem((2, block, rows), BF16),
        vmem((block, wide), BF16),
        vmem((block, rows), BF16),
        vmem((units, block), BF16),
        vmem((block, units), BF16),
        vmem((seqs, rows, hd), BF16),
        vmem((block, 128), BF16),
        vmem((ntp, cols, batch), BF16),
        vmem((nkv, seqs, wide), BF16),
        vmem((nkv, seqs, wide), BF16),
        vmem((seqs, hd), BF16),
        vmem((ntp // 2, seqs, hd), BF16),
        vmem((seqs, rows), BF16),
        vmem((nkv, seqs, rows), BF16),
        vmem((ntp, cols + 2, batch), BF16),
        vmem((ntp, cols + 2, batch), BF16),
        vmem((cols, batch), BF16),
        vmem((ntp, cols, batch), BF16),
        vmem((nkv, share + 2, batch), BF16),
        vmem((nkv, share + 2, batch), BF16),
        vmem((share, batch), BF16),
        vmem((nkv, share, batch), BF16),
        vmem((ntp, cols, batch), BF16),
        vmem((ntp, cols, batch), BF16),
        pltpu.SemaphoreType.DMA((16,)),
        pltpu.SemaphoreType.DMA((14,)),
        pltpu.SemaphoreType.DMA((14,)),
    ]
    anywhere = pl.BlockSpec(memory_space=pl.ANY)
    in_vmem = pl.BlockSpec(memory_space=pltpu.VMEM)
    shapes = (
        ((cols, batch), BF16),
        (cell_state.shape, F32),
        (norm_state.shape, F32),
        (max_state.shape, F32),
    )
    results = pl.pallas_call(
        functools.partial(kernel, nkv, ntp, width),
        out_shape=tuple(pltpu.VMEM(shape, dtype) for shape, dtype in shapes),
        in_specs=[pl.BlockSpec(memory_space=pltpu.HBM)] * len(operands),
        out_specs=(in_vmem,) * 4,
        scratch_shapes=scratch,
        compiler_params=pltpu.CompilerParams(
            collective_id=0, has_side_effects=True, vmem_limit_bytes=24 * 1024 * 1024
        ),
        name="decode_step",
    )(*[pltpu.with_memory_space_constraint(x, pltpu.HBM) for x in operands])
    out, cell_next, norm_next, max_next = pl.pallas_call(
        write_out,
        out_shape=tuple(jax.ShapeDtypeStruct(shape, dtype) for shape, dtype in shapes),
        in_specs=[anywhere] * 4,
        out_specs=(anywhere,) * 4,
        scratch_shapes=[pltpu.SemaphoreType.DMA((4,))],
        compiler_params=pltpu.CompilerParams(vmem_limit_bytes=2 * 1024 * 1024),
        name="write_out",
    )(*results)
    return out.T, cell_next, norm_next, max_next


def solution(mesh):
    kv_tp = ("kv", "tp")
    in_specs = (
        P(None, kv_tp),
        P(),
        P("kv", "tp"),
        P("kv", "tp"),
        P("kv", "tp"),
        P("kv", "tp"),
        P("kv", None),
        P(),
        P("kv", "tp", None),
        P("kv", None, None),
        P("kv", None),
        P(),
        P("tp", "kv"),
        P(),
        P("kv", "tp"),
        P("tp", "kv"),
    )
    out_specs = (P(None, kv_tp), P("kv", "tp", None), P("kv", None, None), P("kv", None))
    body = functools.partial(per_device, mesh.shape["kv"], mesh.shape["tp"])
    return jax.shard_map(
        body, mesh=mesh, in_specs=in_specs, out_specs=out_specs, check_vma=False
    )
```

time: 78.6 us -> 71 us (0.903)
  local copies, waits for them, and re-layouts: 4.83 us -> 0 us
  Pallas kernels: 72.9 us -> 70.2 us
    unnamed x10 -> x0, local copies, waits for them, and re-layouts: 4.83 us -> none
    pallas_call x1 -> x2, Pallas kernels: 72.9 us -> 70.2 us  [the longest x1 69.2 us: per_device(): pl.pallas_call(functools.partial(kernel, nkv, ntp, width), out_shape=tupl...]
where the time goes in v2:
time: 71 us; the launch traced here: 70.9 us
  Pallas kernels  70.2 us (99%)
    pallas_call x1, Pallas kernels, per_device(): pl.pallas_call(functools.partial(kernel, nkv, ntp, width), out_shape=tupl...  69.2 us

profile of v2, /device:TPU:1, one launch (start us, length us, event | category | flops | bytes accessed | tf_op | source)
XLA Modules:
  0.0 70.9 jit_solution(12351013624534361146)
XLA Ops:
  0.6 69.2 %decode_step.1 = (bf16[8,128]{1,0:T(8,128)(2,1)S(1)}, f32[8,128,256]{2,1,0:T(8,128)S(1)}, f32[8,16,256]{2,1,0:T(8,128)S(1)}, f32[8,16]{1,0:T(8,128)S(1)}) custom-call(bf16[8,128]{1,0:T(8,128)(2,1)} %bitcast.11, f32[32,128]{1,0:T(8,128)} %bitcast.7, bf16[256,128]{1,0:T(8,128)(2,1)} %wq_ref.1, bf16[256,128]{1,0:T(8,128)(2,1)} %wk_ref.1, ...), custom_call_target="tpu_custom_call" | custom-call | tf_op jit(solution)/shard_map/decode_step/pallas_call | solution.py:523
  69.8 1.0 %write_out.1 = (bf16[8,128]{1,0:T(8,128)(2,1)}, f32[8,128,256]{2,1,0:T(8,128)}, f32[8,16,256]{2,1,0:T(8,128)}, f32[8,16]{1,0:T(8,128)}) custom-call(bf16[8,128]{1,0:T(8,128)(2,1)S(1)} %get-tuple-element.12.refs_0_, f32[8,128,256]{2,1,0:T(8,128)S(1)} %get-tuple-element.13.refs_1_, f32[8,16,256]{2,1,0:T(8,128)S(1)} %get-tuple-element.14.refs_2_, ...), custom_call_target="tpu_custom_call" | custom-call | tf_op jit(solution)/shard_map/write_out/pallas_call | solution.py:534
